TPU v7x, 32 devices: a whole 2x2x4 slice. The times are simulated.
32 devices in a mesh: grp: 2 (over y), ep: 4 (over z), tp: 4 (over x, core).
Axes of the slice: x: 2, y: 2, z: 4, core: 2. Of those that a mesh axis runs over, the one named last changes fastest.
Arguments:
- queries: bfloat16 [1024, 16, 128], P(('grp', 'ep'), 'tp'), parts along dimension 0, may hold values from -6 to 6
- key_vectors: bfloat16 [1024, 16, 128], P(('grp', 'ep'), 'tp'), parts along dimension 0, may hold values from -6 to 6
- values: bfloat16 [1024, 16, 128], P(('grp', 'ep'), 'tp'), parts along dimension 0, may hold values from -6 to 6
- forget_cum: float32 [1024, 16], P('grp', 'tp'), parts along dimension 0, may hold values from -90 to 0, as said below
- query_gain: float32 [128], replicated, may hold values from 0.1 to 5.5
- key_gain: float32 [128], replicated, may hold values from 0.1 to 5.5
- tokens: bfloat16 [4096, 4096], P(('grp', 'ep', 'tp')), parts along dimension 0, may hold values from -6 to 6
- norm_gain: float32 [4096], replicated, may hold values from 0.1 to 1.9
- routes: int32 [4096, 2], P(('grp', 'ep', 'tp')), parts along dimension 0, may hold values from 0 to 127, all different within a row; in each aligned block of 128 rows (0 to 127, 128 to 255, ...) at most 2 rows name the same one
- route_weights: float32 [4096, 2], P(('grp', 'ep', 'tp')), parts along dimension 0, may hold values from 0.3 to 1.2
- expert_gate: bfloat16 [128, 4096, 384], P(('ep', 'tp')), may hold values from -0.09375 to 0.09375
- expert_up: bfloat16 [128, 4096, 384], P(('ep', 'tp')), may hold values from -0.09375 to 0.09375
- expert_down: bfloat16 [128, 384, 4096], P(('ep', 'tp')), may hold values from -0.3125 to 0.3125
- shared_gate: bfloat16 [4096, 192], P(None, 'tp'), may hold values from -0.09375 to 0.09375
- shared_up: bfloat16 [4096, 192], P(None, 'tp'), may hold values from -0.09375 to 0.09375
- shared_down: bfloat16 [192, 4096], P('tp'), may hold values from -0.4375 to 0.4375
Outputs:
- attended: bfloat16 [1024, 16, 128], P(('grp', 'ep'), 'tp'), parts along dimension 0
- routed_output: bfloat16 [4096, 4096], P(('grp', 'ep', 'tp')), parts along dimension 0
There are 2 independent parts, one for each index of `grp`. A program takes and returns all parts, laid end to end along the dimension named above; an argument that names none is the same for every part. Nothing has to cross between parts.
Inputs may be any that keep to these rules, and one draw needn't show every extreme that they name: `routes`: each row names 2 different experts; the rows of one device name every expert exactly 2 times. `forget_cum`: never rises from one position to the next.
All inputs are finite; a program needn't handle non-finite values.
Results may differ from a plain program's by a relative error of at most 0.007.
The roundings to bfloat16 on the way count: a program that leaves them out, or rounds other values in their place, can miss the bound.
Values may be sent and summed in bfloat16 or wider, within the bound.
A program may use at most 128 MiB of HBM per device.

v0:
```python
import jax
import jax.numpy as jnp
from jax import lax
from jax.sharding import PartitionSpec as P

D = 4096
EXPERTS = 128
TOP_K = 2
CAP = 2


def rms_rows(row_values, gain_vector):
    widened = row_values.astype(jnp.float32)
    inverse = lax.rsqrt(jnp.mean(widened * widened, axis=-1, keepdims=True) + 1e-06)
    return (widened * inverse * gain_vector).astype(jnp.bfloat16)


def attend(queries, key_vectors, values, forget_cum, query_gain, key_gain):
    query_norm = rms_rows(queries, query_gain)
    key_norm = rms_rows(key_vectors, key_gain)
    query_rows = query_norm.shape[0]
    head_count = query_norm.shape[1]
    head_size = query_norm.shape[2]
    first_query = lax.axis_index("ep") * query_rows
    query_positions = first_query + lax.iota(jnp.int32, query_rows)
    last_query = first_query + query_rows - 1
    query_cum = lax.dynamic_slice_in_dim(forget_cum, first_query, query_rows, 0).T
    scale_factor = head_size ** (-0.5)
    start_state = (
        jnp.full((head_count, query_rows), -1e30, jnp.float32),
        jnp.zeros((head_count, query_rows), jnp.float32),
        jnp.zeros((head_count, query_rows, head_size), jnp.float32),
    )
    key_part = lax.all_gather(key_norm, "ep", axis=0, tiled=True)
    value_part = lax.all_gather(values, "ep", axis=0, tiled=True)
    piece_rows = key_part.shape[0]

    def compute(inner_state):
        best_score, denominator, accumulated = inner_state
        cum_block = forget_cum.T
        scores = jnp.einsum(
            "qhd,khd->hqk", query_norm, key_part, preferred_element_type=jnp.float32
        )
        scores = scores * scale_factor + query_cum[:, :, None] - cum_block[:, None, :]
        key_positions = lax.iota(jnp.int32, piece_rows)
        allowed = (key_positions[None, :] <= query_positions[:, None])[None]
        scores = jnp.where(allowed, scores, -1e30)
        new_best = jnp.maximum(best_score, jnp.max(scores, axis=2))
        weights = jnp.where(allowed, jnp.exp(scores - new_best[:, :, None]), 0.0)
        denominator = jnp.sum(weights, axis=2)
        product = jnp.einsum(
            "hqk,khd->hqd",
            weights.astype(jnp.bfloat16),
            value_part,
            preferred_element_type=jnp.float32,
        )
        accumulated = product
        return (new_best, denominator, accumulated)

    best_score, denominator, accumulated = lax.cond(
        jnp.int32(0) <= last_query, compute, lambda inner_state: inner_state, start_state
    )
    return (accumulated / denominator[:, :, None]).transpose(1, 0, 2).astype(jnp.bfloat16)


def shared_expert(normed, shared_gate, shared_up, shared_down):
    row_count = normed.shape[0]
    whole_gate, whole_up, whole_down = (
        lax.all_gather(shared_gate, "tp", axis=1, tiled=True),
        lax.all_gather(shared_up, "tp", axis=1, tiled=True),
        lax.all_gather(shared_down, "tp", axis=0, tiled=True),
    )
    block_total = lax.axis_size("tp")
    gate_values = jnp.dot(normed, whole_gate, preferred_element_type=jnp.float32)
    upward = jnp.dot(normed, whole_up, preferred_element_type=jnp.float32)
    hidden_whole = (jax.nn.silu(gate_values) * upward).astype(jnp.bfloat16)
    part_width = whole_down.shape[0] // block_total
    hidden_blocks = hidden_whole.reshape(row_count, block_total, part_width)
    down_blocks = whole_down.reshape(block_total, part_width, whole_down.shape[1])
    partials = jnp.einsum(
        "rnp,npd->nrd", hidden_blocks, down_blocks, preferred_element_type=jnp.float32
    ).astype(jnp.bfloat16)
    return jnp.sum(partials.astype(jnp.float32), axis=0).astype(jnp.bfloat16)


def mixture(
    tokens,
    norm_gain,
    routes,
    route_weights,
    expert_gate,
    expert_up,
    expert_down,
    shared_gate,
    shared_up,
    shared_down,
):
    normed = rms_rows(tokens, norm_gain)
    row_count = tokens.shape[0]
    shared_out = shared_expert(normed, shared_gate, shared_up, shared_down)
    flat_routes = routes.reshape(-1)
    choice_count = flat_routes.shape[0]
    one_hot = (flat_routes[:, None] == lax.iota(jnp.int32, EXPERTS)[None, :]).astype(jnp.int32)
    slot_rank = jnp.sum((jnp.cumsum(one_hot, axis=0) - one_hot) * one_hot, axis=1)
    slot_index = slot_rank * EXPERTS + flat_routes
    slot_ids = lax.iota(jnp.int32, CAP * EXPERTS)
    matches = slot_index[None, :] == slot_ids[:, None]
    source_row = jnp.sum(
        jnp.where(matches, lax.iota(jnp.int32, choice_count)[None, :] // TOP_K, 0), axis=1
    )
    filled = jnp.any(matches, axis=1)
    outgoing = jnp.where(filled[:, None], normed[source_row], jnp.zeros((), jnp.bfloat16)).reshape(
        CAP, EXPERTS, D
    )
    arrived = lax.all_to_all(outgoing, ("ep", "tp"), split_axis=1, concat_axis=1, tiled=True)
    local_count = expert_gate.shape[0]
    grouped = arrived.reshape(CAP, -1, local_count, D)
    gate_values = jnp.einsum(
        "csed,edf->csef", grouped, expert_gate, preferred_element_type=jnp.float32
    )
    upward = jnp.einsum("csed,edf->csef", grouped, expert_up, preferred_element_type=jnp.float32)
    hidden = (jax.nn.silu(gate_values) * upward).astype(jnp.bfloat16)
    produced = (
        jnp.einsum("csef,efd->csed", hidden, expert_down, preferred_element_type=jnp.float32)
        .astype(jnp.bfloat16)
        .reshape(CAP, -1, D)
    )
    returned = lax.all_to_all(produced, ("ep", "tp"), split_axis=1, concat_axis=1, tiled=True)
    picked_rows = returned.reshape(CAP * EXPERTS, D)[slot_index].reshape(row_count, TOP_K, D)
    routed = jnp.sum(route_weights[:, :, None] * picked_rows.astype(jnp.float32), axis=1)
    return (shared_out.astype(jnp.float32) + routed).astype(jnp.bfloat16)


def local(
    queries,
    key_vectors,
    values,
    forget_cum,
    query_gain,
    key_gain,
    tokens,
    norm_gain,
    routes,
    route_weights,
    expert_gate,
    expert_up,
    expert_down,
    shared_gate,
    shared_up,
    shared_down,
):
    attended = attend(queries, key_vectors, values, forget_cum, query_gain, key_gain)
    routed_output = mixture(
        tokens,
        norm_gain,
        routes,
        route_weights,
        expert_gate,
        expert_up,
        expert_down,
        shared_gate,
        shared_up,
        shared_down,
    )
    return (attended, routed_output)


def solution(mesh):
    placed = (
        P(("grp", "ep"), "tp", None),
        P(("grp", "ep"), "tp", None),
        P(("grp", "ep"), "tp", None),
        P("grp", "tp"),
        P(),
        P(),
        P(("grp", "ep", "tp"), None),
        P(),
        P(("grp", "ep", "tp"), None),
        P(("grp", "ep", "tp"), None),
        P(("ep", "tp"), None, None),
        P(("ep", "tp"), None, None),
        P(("ep", "tp"), None, None),
        P(None, "tp"),
        P(None, "tp"),
        P("tp", None),
    )
    return jax.shard_map(
        local,
        mesh=mesh,
        in_specs=placed,
        out_specs=(P(("grp", "ep"), "tp", None), P(("grp", "ep", "tp"), None)),
        check_vma=False,
    )
```

profile of v0, /device:TPU:0, one launch (start us, length us, event | category | flops | bytes accessed | tf_op | source)
XLA Modules:
  0.0 230.9 jit_solution(5048719747301511845)
XLA Ops:
  7.2 0.9 copy.80
  8.1 0.1 eq.42
  8.2 0.1 eq.38
  8.3 0.1 copy.82
  8.5 0.2 fusion.67
  8.8 0.2 fusion.69
  9.0 0.1 fusion.65
  9.1 0.1 select_reduce_fusion
  9.2 1.5 fusion.23
  10.8 0.1 copy.84
  10.9 0.3 fusion.25
  11.2 1.8 gather_fusion
  13.1 3.8 %broadcast_select_fusion = bf16[2,128,4096]{2,0,1:T(2,128)(2,1)} fusion(pred[2,128]{0,1:T(8,128)(4,1)S(1)} %copy.84, bf16[2,128,4096]{2,1,0:T(8,128)(2,1)S(1)} %bitcast.86), kind=kLoop, calls=%fused_computation.27 | loop fusion | flops 1048576 | bytes 4194560 | tf_op jit(solution)/shard_map/jit(_where)/select_n | solution.py:112
  16.9 7.4 %all-to-all-start = ((bf16[2,128,4096]{2,0,1:T(2,128)(2,1)}), bf16[2,128,4096]{2,0,1:T(2,128)(2,1)}, u32[]{:S(2)}, u32[]{:S(2)}) async-start(bf16[2,128,4096]{2,0,1:T(2,128)(2,1)} %broadcast_select_fusion), calls=%async_computation | async-start | bytes 4194304 | tf_op jit(solution)/shard_map/all_to_all | solution.py:115
  24.4 0.7 all-gather.4.cloned.1.call-update
  25.1 0.2 all-gather.6.cloned.1.call-start
  25.3 0.5 all-gather.6.cloned.1.call-update
  25.9 39.6 %all-to-all-done = bf16[2,128,4096]{2,0,1:T(2,128)(2,1)} async-done(((bf16[2,128,4096]{2,0,1:T(2,128)(2,1)}), bf16[2,128,4096]{2,0,1:T(2,128)(2,1)}, u32[]{:S(2)}, u32[]{:S(2)}) %all-to-all-start) | async-done | bytes 2097184 | tf_op jit(solution)/shard_map/all_to_all | solution.py:115
  65.5 2.9 %copy.120 = bf16[2,128,4096]{2,1,0:T(8,128)(2,1)S(1)} copy(bf16[2,128,4096]{2,0,1:T(2,128)(2,1)} %all-to-all-done) | data formatting | bytes 4194304 | tf_op jit(solution)/shard_map/all_to_all | solution.py:115
  68.4 10.7 %fusion.29 = f32[2,16,8,384]{3,1,0,2:T(8,128)S(1)} fusion(bf16[8,4096,384]{2,1,0:T(8,128)(2,1)} %param.28, bf16[2,16,8,4096]{3,2,1,0:T(8,128)(2,1)S(1)} %bitcast.84), kind=kOutput, calls=%fused_computation.39 | convolution fusion | flops 805306368 | bytes 27656192 | tf_op jit(solution)/shard_map/csed,edf->csef/dot_general | solution.py:118
  79.1 21.4 %fusion.20 = bf16[2,16,8,4096]{3,1,0,2:T(8,128)(2,1)} fusion(bf16[8,384,4096]{2,1,0:T(8,128)(2,1)} %param.30, bf16[8,4096,384]{2,1,0:T(8,128)(2,1)} %param.29, bf16[2,16,8,4096]{3,2,1,0:T(8,128)(2,1)S(1)} %bitcast.85, f32[2,16,8,384]{3,1,0,2:T(8,128)S(1)} %fusion.29), kind=kOutput, calls=%fused_computation.25 | convolution fusion | flops 1612251136 | bytes 54919168 | tf_op jit(solution)/shard_map/csef,efd->csed/dot_general | solution.py:124
  100.5 2.7 %copy.119 = bf16[2,16,8,4096]{3,2,1,0:T(8,128)(2,1)S(1)} copy(bf16[2,16,8,4096]{3,1,0,2:T(8,128)(2,1)} %fusion.20) | data formatting | bytes 4194304 | tf_op jit(solution)/shard_map/convert_element_type | solution.py:125
  103.3 3.5 %copy.90 = bf16[2,128,4096]{2,0,1:T(2,128)(2,1)} copy(bf16[2,128,4096]{2,1,0:T(8,128)(2,1)S(1)} %bitcast.87) | data formatting | bytes 4194304 | tf_op jit(solution)/shard_map/reshape | solution.py:126
  106.8 11.5 %all-to-all-start.1 = ((bf16[2,128,4096]{2,0,1:T(2,128)(2,1)}), bf16[2,128,4096]{2,0,1:T(2,128)(2,1)}, u32[]{:S(2)}, u32[]{:S(2)}) async-start(bf16[2,128,4096]{2,0,1:T(2,128)(2,1)} %copy.90), calls=%async_computation.1 | async-start | bytes 4194304 | tf_op jit(solution)/shard_map/all_to_all | solution.py:128
  118.3 0.3 all-gather.8.cloned.1.call-start
  118.5 0.5 all-gather.8.cloned.1.call-update
  119.0 0.1 reshape.194
  119.4 0.1 fusion.62
  119.5 0.1 fusion.59
  119.7 0.1 fusion.64
  119.8 57.6 %all_gather.15 = bf16[512,4,128]{2,0,1:T(8,128)(2,1)S(1)} all-gather(bf16[128,4,128]{2,0,1:T(8,128)(2,1)S(1)} %fusion.64), channel_id=1, replica_groups=mesh['grp'=2,'ep'=4,'tp'=4] {'ep'}, dimensions={0}, use_global_device_ids=true | all-gather | bytes 655360 | tf_op jit(solution)/shard_map/all_gather | solution.py:34
  177.5 15.9 %all_gather.16 = bf16[512,4,128]{2,0,1:T(8,128)(2,1)S(1)} all-gather(bf16[128,4,128]{2,0,1:T(8,128)(2,1)S(1)} %copy.76), channel_id=1, replica_groups=mesh['grp'=2,'ep'=4,'tp'=4] {'ep'}, dimensions={0}, use_global_device_ids=true | all-gather | bytes 655360 | tf_op jit(solution)/shard_map/all_gather | solution.py:35
  193.4 0.1 fusion.61
  193.5 1.5 conditional.1
  193.6 0.5 fusion.75
  194.1 0.4 fusion.5
  194.5 0.2 copy.97
  194.7 0.3 fusion.4
  195.0 0.1 copy.77
  195.2 0.9 fusion.71
  196.0 2.0 fusion.76
  198.0 2.0 fusion.53
  200.1 2.8 %fusion.28 = bf16[128,4096]{1,0:T(8,128)(2,1)S(1)} fusion(bf16[128,4,48]{0,2,1:T(8,128)(2,1)S(1)} %bitcast.90, bf16[4,48,4096]{2,1,0:T(8,128)(2,1)} %bitcast.98), kind=kOutput, calls=%fused_computation.38 | convolution fusion | flops 204996608 | bytes 2670592 | tf_op jit(solution)/shard_map/rnp,npd->nrd/dot_general | solution.py:80
  202.9 2.9 %copy.91 = bf16[2,128,4096]{2,1,0:T(8,128)(2,1)S(1)} copy(bf16[2,128,4096]{2,0,1:T(2,128)(2,1)} %all-to-all-done.1) | data formatting | bytes 4194304 | tf_op jit(solution)/shard_map/all_to_all | solution.py:128
  205.8 3.2 %gather_fusion.1 = bf16[256,4096]{1,0:T(8,128)(2,1)} fusion(bf16[256,4096]{1,0:T(8,128)(2,1)S(1)} %bitcast.83, s32[1024]{0:T(1024)S(1)} %pad_clamp_fusion), kind=kCustom, calls=%fused_computation.1 | custom fusion | bytes 4195328 | tf_op jit(solution)/shard_map/gather | solution.py:129
  209.0 5.4 %reshape.195 = f32[128,2,4096]{2,1,0:T(2,128)} reshape(bf16[256,4096]{1,0:T(8,128)(2,1)} %gather_fusion.1) | data formatting | bytes 6291456 | tf_op jit(solution)/shard_map/convert_element_type | solution.py:130
  214.4 8.7 %multiply_reduce_fusion = f32[128,4096]{1,0:T(8,128)S(1)} fusion(f32[128,2,4096]{2,1,0:T(2,128)} %reshape.195, f32[128,2]{1,0:T(8,128)S(1)} %copy.79), kind=kLoop, calls=%fused_computation.26 | loop fusion | flops 1572864 | bytes 6292480 | tf_op jit(solution)/shard_map/reduce_sum | solution.py:130
  223.2 1.2 add_convert_fusion
  (48 shorter events, 0.5 us)
Async XLA Ops:
  7.2 3.7 %copy-start = (bf16[128,4096]{1,0:T(8,128)(2,1)S(1)}, bf16[128,4096]{1,0:T(8,128)(2,1)}, u32[]{:S(2)}) copy-start(bf16[128,4096]{1,0:T(8,128)(2,1)} %param.24) | copy-start | bytes 3145732
  7.2 3.7 %copy-start.6 = (f32[4096]{0:T(1024)S(1)}, f32[4096]{0:T(1024)}, u32[]{:S(2)}) copy-start(f32[4096]{0:T(1024)} %param.25) | copy-start | bytes 49156
  8.1 2.7 %copy-start.1 = (s32[128,2]{1,0:T(8,128)}, s32[128,2]{1,0:T(8,128)S(1)}, u32[]{:S(2)}) copy-start(s32[128,2]{1,0:T(8,128)S(1)} %copy.80) | copy-start | bytes 3076
  16.9 48.5 %all-to-all-start = ((bf16[2,128,4096]{2,0,1:T(2,128)(2,1)}), bf16[2,128,4096]{2,0,1:T(2,128)(2,1)}, u32[]{:S(2)}, u32[]{:S(2)}) async-start(bf16[2,128,4096]{2,0,1:T(2,128)(2,1)} %broadcast_select_fusion), calls=%async_computation | async-start | bytes 4194304 | tf_op jit(solution)/shard_map/all_to_all | solution.py:115
  24.4 171.6 %all-gather.4.cloned.1.call-start = ((), (), s32[]{:S(2)}) async-start(), calls=%async_computation.2 | async-start | bytes 1966080 | tf_op jit(solution)/shard_map/all_gather | solution.py:69
  25.1 172.9 %all-gather.6.cloned.1.call-start = ((), (), s32[]{:S(2)}) async-start(), calls=%async_computation.3 | async-start | bytes 1966080 | tf_op jit(solution)/shard_map/all_gather | solution.py:70
  106.8 12.3 %copy-start.2 = (s32[128,2]{1,0:T(8,128)S(1)}, s32[128,2]{1,0:T(8,128)}, u32[]{:S(2)}) copy-start(s32[128,2]{1,0:T(8,128)} %copy-done.1) | copy-start | bytes 3076
  106.8 12.4 %copy-start.7 = (f32[128,2]{0,1:T(2,128)S(1)}, f32[128,2]{0,1:T(2,128)}, u32[]{:S(2)}) copy-start(f32[128,2]{0,1:T(2,128)} %param.27) | copy-start | bytes 3076
  106.8 12.5 %copy-start.5 = (bf16[128,4,128]{2,1,0:T(4,128)(2,1)S(1)}, bf16[128,4,128]{2,1,0:T(4,128)(2,1)}, u32[]{:S(2)}) copy-start(bf16[128,4,128]{2,1,0:T(4,128)(2,1)} %param.20) | copy-start | bytes 393220
  106.8 12.6 %copy-start.10 = (f32[512,4]{0,1:T(4,128)S(1)}, f32[512,4]{0,1:T(4,128)}, u32[]{:S(2)}) copy-start(f32[512,4]{0,1:T(4,128)} %param.21) | copy-start | bytes 24580
  106.8 12.6 %copy-start.3 = (bf16[128,4,128]{2,1,0:T(4,128)(2,1)S(1)}, bf16[128,4,128]{2,1,0:T(4,128)(2,1)}, u32[]{:S(2)}) copy-start(bf16[128,4,128]{2,1,0:T(4,128)(2,1)} %param.19) | copy-start | bytes 393220
  106.8 12.7 %copy-start.4 = (bf16[128,4,128]{2,1,0:T(4,128)(2,1)S(1)}, bf16[128,4,128]{2,1,0:T(4,128)(2,1)}, u32[]{:S(2)}) copy-start(bf16[128,4,128]{2,1,0:T(4,128)(2,1)} %param.18) | copy-start | bytes 393220
  106.8 12.9 %copy-start.8 = (f32[128]{0:T(128)S(1)}, f32[128]{0:T(128)}, u32[]{:S(2)}) copy-start(f32[128]{0:T(128)} %param.23) | copy-start | bytes 1540
  106.8 96.0 %all-to-all-start.1 = ((bf16[2,128,4096]{2,0,1:T(2,128)(2,1)}), bf16[2,128,4096]{2,0,1:T(2,128)(2,1)}, u32[]{:S(2)}, u32[]{:S(2)}) async-start(bf16[2,128,4096]{2,0,1:T(2,128)(2,1)} %copy.90), calls=%async_computation.1 | async-start | bytes 4194304 | tf_op jit(solution)/shard_map/all_to_all | solution.py:128
  118.3 75.1 %copy-start.9 = (f32[128]{0:T(128)S(1)}, f32[128]{0:T(128)}, u32[]{:S(2)}) copy-start(f32[128]{0:T(128)} %param.22) | copy-start | bytes 1540
  118.3 81.8 %all-gather.8.cloned.1.call-start = ((), (), s32[]{:S(2)}) async-start(), calls=%async_computation.4 | async-start | bytes 1966080 | tf_op jit(solution)/shard_map/all_gather | solution.py:71
Sparse Core Ops, SparseCore 0:
  26.8 28.5 all-gather.3
  56.9 20.2 all-gather.5
  120.6 28.3 all-gather.7
where the time goes:
time: 231 us
  blocking collectives  73.5 us (32%)
  waiting for transfers between devices  41.3 us (18%)
  matrix products  39.7 us (17%)
  local copies, waits for them, and re-layouts  24.6 us (11%)
  starting transfers between devices  19.4 us (8%)
  other arithmetic  18.3 us (8%)
  between operations  14.1 us (6%)
    all_gather x1, blocking collectives, attend(): key_part = lax.all_gather(key_norm, 'ep', axis=0, tiled=True)  57.6 us
    all_to_all x1, waiting for transfers between devices, mixture(): lax.all_to_all(outgoing, ('ep', 'tp'), split_axis=1, concat_axis=1, tiled...  39.6 us
    dot_general x1, matrix products, mixture(): jnp.einsum('csef,efd->csed', hidden, expert_down, preferred_element_type=...  21.4 us
    all_gather x1, blocking collectives, attend(): value_part = lax.all_gather(values, 'ep', axis=0, tiled=True)  15.9 us
    all_to_all x1, starting transfers between devices, mixture(): lax.all_to_all(produced, ('ep', 'tp'), split_axis=1, concat_axis=1, tiled...  11.5 us
    dot_general x1, matrix products, mixture(): jnp.einsum('csed,edf->csef', grouped, expert_gate, preferred_element_type...  10.7 us
    reduce_sum x1, other arithmetic, mixture(): jnp.sum(route_weights[:, :, None] * picked_rows.astype(jnp.float32), axis=1)  8.75 us
    all_to_all x1, starting transfers between devices, mixture(): lax.all_to_all(outgoing, ('ep', 'tp'), split_axis=1, concat_axis=1, tiled...  7.44 us
  transfers between devices with their start and end apart: 5, of which 1 were waited for; matrix products, arithmetic and copies ran while one was open for 22% of the time, Pallas kernels for 0%

commit v1 on v0

--- a/solution.py
+++ b/solution.py
@@ -1,12 +1,21 @@
+import functools
 import jax
 import jax.numpy as jnp
 from jax import lax
+from jax.experimental import pallas as pl
+from jax.experimental.pallas import tpu as pltpu
 from jax.sharding import PartitionSpec as P
+
+MESH = pl.DeviceIdType.MESH
+F32 = jnp.float32
+BF16 = jnp.bfloat16
+CAP = 2
+CHUNKS = 4
+SLOTS = 4
 
 D = 4096
 EXPERTS = 128
 TOP_K = 2
-CAP = 2
 
 
 def rms_rows(row_values, gain_vector):
@@ -165,6 +174,581 @@
     return (attended, routed_output)
 
 
+def rms_heads(wide, gain, heads, size):
+    pieces = []
+    for h in range(heads):
+        part = wide[:, h * size : (h + 1) * size]
+        inverse = lax.rsqrt(jnp.mean(part * part, axis=-1, keepdims=True) + 1e-06)
+        pieces.append((part * inverse * gain).astype(BF16))
+    return jnp.concatenate(pieces, axis=1)
+
+
+def prepare_kernel(
+    local_count,
+    heads,
+    tokens_ref,
+    gain_ref,
+    routes_ref,
+    routes_t_ref,
+    weights_ref,
+    q_ref,
+    k_ref,
+    qg_ref,
+    kg_ref,
+    normed_ref,
+    out_ref,
+    high_ref,
+    low_ref,
+    qn_ref,
+    kn_ref,
+):
+    size = qg_ref.shape[1]
+    qn_ref[...] = rms_heads(q_ref[...].astype(F32), qg_ref[...], heads, size)
+    kn_ref[...] = rms_heads(k_ref[...].astype(F32), kg_ref[...], heads, size)
+    rows = tokens_ref.shape[0]
+    slots = out_ref.shape[0]
+    group = CAP * local_count
+
+    def expert_of(r):
+        return (r // group) * local_count + r % local_count
+
+    def rank_of(r):
+        return ((r % group) // local_count).astype(F32)
+
+    r = lax.broadcasted_iota(jnp.int32, (slots, rows), 0)
+    expert = expert_of(r)
+    named = (expert == routes_t_ref[0:1, :]) | (expert == routes_t_ref[1:2, :])
+    named = jnp.where(named, 1.0, 0.0)
+    a = lax.broadcasted_iota(jnp.int32, (rows, rows), 0)
+    b = lax.broadcasted_iota(jnp.int32, (rows, rows), 1)
+    before = jnp.where(a < b, 1.0, 0.0).astype(BF16)
+    earlier = jnp.dot(named.astype(BF16), before, preferred_element_type=F32)
+    pick = jnp.where(earlier == rank_of(r), named, 0.0).astype(BF16)
+    r = lax.broadcasted_iota(jnp.int32, (rows, slots), 1)
+    expert = expert_of(r)
+    first = expert == routes_ref[:, 0:1]
+    second = expert == routes_ref[:, 1:2]
+    named = jnp.where(first | second, 1.0, 0.0)
+    after = jnp.where(b < a, 1.0, 0.0).astype(BF16)
+    earlier = jnp.dot(after, named.astype(BF16), preferred_element_type=F32)
+    weight = jnp.where(first, weights_ref[:, 0:1], weights_ref[:, 1:2])
+    weight = jnp.where(earlier == rank_of(r), named * weight, 0.0)
+    high = weight.astype(BF16)
+    high_ref[...] = high
+    low_ref[...] = (weight - high.astype(F32)).astype(BF16)
+
+    wide = tokens_ref[...].astype(F32)
+    inverse = lax.rsqrt(jnp.mean(wide * wide, axis=-1, keepdims=True) + 1e-06)
+    width = tokens_ref.shape[1] // 8
+    for c in range(8):
+        cols = slice(c * width, (c + 1) * width)
+        piece = (tokens_ref[:, cols].astype(F32) * inverse * gain_ref[:, cols]).astype(BF16)
+        normed_ref[:, cols] = piece
+        out_ref[:, cols] = jnp.dot(pick, piece, preferred_element_type=F32).astype(BF16)
+
+
+def fused_kernel(
+    n_ep,
+    n_tp,
+    heads,
+    normed_ref,
+    high_ref,
+    low_ref,
+    qn_ref,
+    qc_ref,
+    kc_ref,
+    outgoing_ref,
+    kn_ref,
+    v_ref,
+    gate_ref,
+    up_ref,
+    down_ref,
+    shared_ref,
+    att_ref,
+    res_ref,
+    x_buf,
+    y_buf,
+    r_buf,
+    ring,
+    down_buf,
+    sh_buf,
+    kv_buf,
+    acc_g,
+    acc_u,
+    hid,
+    sh_out,
+    x_send,
+    x_recv,
+    x_own,
+    y_send,
+    y_recv,
+    y_own,
+    ring_sem,
+    down_sem,
+    sh_send,
+    sh_recv,
+    sh_own,
+    sf_send,
+    sf_recv,
+    kv_send,
+    kv_recv,
+    kv_own,
+):
+    e_pos = lax.axis_index("ep")
+    t_pos = lax.axis_index("tp")
+    count = n_ep * n_tp
+    me = e_pos * n_tp + t_pos
+    local_count = gate_ref.shape[0]
+    group = CAP * local_count
+    slots = count * group
+    wide = x_buf.shape[2]
+    steps = CHUNKS * local_count
+    peer_rows = (count - 1) * group
+
+    def device(i):
+        return {"ep": i // n_tp, "tp": i % n_tp}
+
+    def weight_copies(n, slot):
+        rows = pl.ds(pl.multiple_of((n // local_count) * wide, wide), wide)
+        e = n % local_count
+        return (
+            pltpu.make_async_copy(gate_ref.at[e, rows], ring.at[slot, 0], ring_sem.at[slot, 0]),
+            pltpu.make_async_copy(up_ref.at[e, rows], ring.at[slot, 1], ring_sem.at[slot, 1]),
+        )
+
+    barrier = pltpu.get_barrier_semaphore()
+
+    def greet(i, carry):
+        pl.semaphore_signal(
+            barrier, inc=1, device_id=device((me + i) % count), device_id_type=MESH
+        )
+        return carry
+
+    lax.fori_loop(1, count, greet, 0)
+    for n in range(SLOTS):
+        for copy in weight_copies(n, n):
+            copy.start()
+    down_copy = pltpu.make_async_copy(down_ref, down_buf, down_sem)
+    down_copy.start()
+    own_kv = [
+        pltpu.make_async_copy(src, kv_buf.at[e_pos, j], kv_own.at[j])
+        for j, src in enumerate((kn_ref, v_ref))
+    ]
+    for copy in own_kv:
+        copy.start()
+    own_shared = pltpu.make_async_copy(shared_ref, sh_buf.at[t_pos], sh_own)
+    own_shared.start()
+    for blk in range(n_ep):
+
+        @pl.when(blk > e_pos)
+        def _():
+            kv_buf[blk] = jnp.zeros(kv_buf.shape[1:], BF16)
+
+    pl.semaphore_wait(barrier, count - 1)
+
+    def rows_of(i):
+        return pl.ds(pl.multiple_of(i * group, group), group)
+
+    def dispatch(c):
+        cols = pl.ds(c * wide, wide)
+        pltpu.make_async_copy(
+            outgoing_ref.at[rows_of(me), cols], x_buf.at[c, rows_of(me)], x_own.at[c]
+        ).start()
+
+        def send(i, carry):
+            peer = (me + i) % count
+            pltpu.make_async_remote_copy(
+                src_ref=outgoing_ref.at[rows_of(peer), cols],
+                dst_ref=x_buf.at[c, rows_of(me)],
+                send_sem=x_send.at[c],
+                recv_sem=x_recv.at[c],
+                device_id=device(peer),
+                device_id_type=MESH,
+            ).start()
+            return carry
+
+        lax.fori_loop(1, count, send, 0)
+
+    def kv_copy(step, src_k, src_v):
+        blk = jnp.maximum(e_pos - step, 0)
+        nxt = jnp.minimum(e_pos + 1, n_ep - 1)
+        return [
+            pltpu.make_async_remote_copy(
+                src_ref=src,
+                dst_ref=kv_buf.at[blk, j],
+                send_sem=kv_send.at[step, j],
+                recv_sem=kv_recv.at[step, j],
+                device_id={"ep": nxt},
+                device_id_type=MESH,
+            )
+            for j, src in enumerate((src_k, src_v))
+        ]
+
+    def kv_arrived(step):
+        blk = jnp.maximum(e_pos - 1 - step, 0)
+
+        @pl.when(e_pos - 1 - step >= 0)
+        def _():
+            for j in range(2):
+                pltpu.make_async_copy(
+                    kv_buf.at[blk, j], kv_buf.at[blk, j], kv_recv.at[step, j]
+                ).wait()
+
+    def kv_forward(step):
+        blk = jnp.maximum(e_pos - step, 0)
+
+        @pl.when((e_pos - step >= 0) & (e_pos + 1 < n_ep))
+        def _():
+            for copy in kv_copy(step, kv_buf.at[blk, 0], kv_buf.at[blk, 1]):
+                copy.start()
+
+    mate = t_pos + 1 - 2 * (t_pos % 2)
+    across = (t_pos + 2) % n_tp
+
+    def shared_first(target, s, c):
+        cols = pl.ds(c * wide, wide)
+        return pltpu.make_async_remote_copy(
+            src_ref=shared_ref.at[:, cols],
+            dst_ref=sh_buf.at[t_pos, :, cols],
+            send_sem=sh_send.at[s, c],
+            recv_sem=sh_recv.at[s, c],
+            device_id={"tp": target},
+            device_id_type=MESH,
+        )
+
+    def shared_send(c):
+        shared_first(mate, 0, c).start()
+        shared_first(across, 1, c).start()
+
+    @pl.when(e_pos + 1 < n_ep)
+    def _():
+        for copy in kv_copy(0, kn_ref, v_ref):
+            copy.start()
+
+    dispatch(0)
+    dispatch(1)
+    shared_send(0)
+    acc_g[...] = jnp.zeros(acc_g.shape, F32)
+    acc_u[...] = jnp.zeros(acc_u.shape, F32)
+    owner = lax.broadcasted_iota(jnp.int32, acc_g.shape, 0) % local_count
+    for c in range(CHUNKS):
+        pltpu.make_async_copy(
+            x_buf.at[c, pl.ds(0, peer_rows)], x_buf.at[c, pl.ds(0, peer_rows)], x_recv.at[c]
+        ).wait()
+        pltpu.make_async_copy(
+            x_buf.at[c, pl.ds(0, group)], x_buf.at[c, pl.ds(0, group)], x_own.at[c]
+        ).wait()
+        if c < n_ep - 2:
+            kv_arrived(c)
+            kv_forward(c + 1)
+        if c + 2 < CHUNKS:
+            dispatch(c + 2)
+            shared_send(c + 1)
+        if c == CHUNKS - 2:
+            shared_send(CHUNKS - 1)
+
+        def one(e, carry):
+            n = c * local_count + e
+            slot = n % SLOTS
+            for copy in weight_copies(n, slot):
+                copy.wait()
+            x = x_buf[c]
+            mine = owner == e
+            g = jnp.dot(x, ring[slot, 0], preferred_element_type=F32)
+            acc_g[...] += jnp.where(mine, g, 0.0)
+            u = jnp.dot(x, ring[slot, 1], preferred_element_type=F32)
+            acc_u[...] += jnp.where(mine, u, 0.0)
+
+            @pl.when(n + SLOTS < steps)
+            def _():
+                for copy in weight_copies(n + SLOTS, slot):
+                    copy.start()
+
+            return carry
+
+        lax.fori_loop(0, local_count, one, 0)
+
+    g = acc_g[...]
+    hidden = (g / (1.0 + jnp.exp(-g))) * acc_u[...]
+    width = acc_g.shape[1]
+    for e in range(local_count):
+        hid[:, e * width : (e + 1) * width] = jnp.where(owner == e, hidden, 0.0).astype(BF16)
+    down_copy.wait()
+
+    for c in range(CHUNKS):
+        cols = pl.ds(c * wide, wide)
+        half = wide // 2
+
+        def tile(i, carry):
+            y_buf[c, :, pl.ds(pl.multiple_of(i * half, half), half)] = jnp.dot(
+                hid[...],
+                down_buf[:, pl.ds(pl.multiple_of(c * wide + i * half, half), half)],
+                preferred_element_type=F32,
+            ).astype(BF16)
+            return carry
+
+        lax.fori_loop(0, 2, tile, 0)
+        pltpu.make_async_copy(
+            y_buf.at[c, rows_of(me)], r_buf.at[c, rows_of(me)], y_own.at[c]
+        ).start()
+
+        def give(i, carry):
+            peer = (me + i) % count
+            pltpu.make_async_remote_copy(
+                src_ref=y_buf.at[c, rows_of(peer)],
+                dst_ref=r_buf.at[c, rows_of(me)],
+                send_sem=y_send.at[c],
+                recv_sem=y_recv.at[c],
+                device_id=device(peer),
+                device_id_type=MESH,
+            ).start()
+            return carry
+
+        lax.fori_loop(1, count, give, 0)
+
+    for step in range(max(n_ep - 2, 0), n_ep - 1):
+        kv_arrived(step)
+    for copy in own_kv:
+        copy.wait()
+
+    across_copies = []
+    for c in range(CHUNKS):
+        cols = pl.ds(c * wide, wide)
+        pltpu.make_async_copy(
+            sh_buf.at[across, :, cols], sh_buf.at[across, :, cols], sh_recv.at[1, c]
+        ).wait()
+        copy = pltpu.make_async_remote_copy(
+            src_ref=sh_buf.at[across, :, cols],
+            dst_ref=sh_buf.at[across, :, cols],
+            send_sem=sf_send.at[c],
+            recv_sem=sf_recv.at[c],
+            device_id={"tp": mate},
+            device_id_type=MESH,
+        )
+        copy.start()
+        across_copies.append(copy)
+
+    size = qn_ref.shape[1] // heads
+    rows = qn_ref.shape[0]
+    length = n_ep * rows
+    at = e_pos * rows + lax.broadcasted_iota(jnp.int32, (rows, length), 0)
+    allowed = lax.broadcasted_iota(jnp.int32, (rows, length), 1) <= at
+    contract = (((1,), (1,)), ((), ()))
+    for h in range(heads):
+        span = slice(h * size, (h + 1) * size)
+        q = qn_ref[:, span]
+        scores = jnp.concatenate(
+            [
+                lax.dot_general(q, kv_buf[blk, 0, :, span], contract, preferred_element_type=F32)
+                for blk in range(n_ep)
+            ],
+            axis=1,
+        )
+        scores = scores * (size**-0.5) + qc_ref[:, h : h + 1] - kc_ref[h : h + 1, :]
+        scores = jnp.where(allowed, scores, -1e30)
+        top = jnp.max(scores, axis=1, keepdims=True)
+        weights = jnp.where(allowed, jnp.exp(scores - top), 0.0)
+        total = jnp.sum(weights, axis=1, keepdims=True)
+        weights = weights.astype(BF16)
+        mixed = jnp.zeros((rows, size), F32)
+        for blk in range(n_ep):
+            mixed += jnp.dot(
+                weights[:, blk * rows : (blk + 1) * rows],
+                kv_buf[blk, 1, :, span],
+                preferred_element_type=F32,
+            )
+        att_ref[:, span] = (mixed / total).astype(BF16)
+
+    own_shared.wait()
+    third = mate + 2 - 4 * (mate // 2)
+    for c in range(CHUNKS):
+        cols = pl.ds(c * wide, wide)
+        pltpu.make_async_copy(
+            sh_buf.at[mate, :, cols], sh_buf.at[mate, :, cols], sh_recv.at[0, c]
+        ).wait()
+        pltpu.make_async_copy(
+            sh_buf.at[third, :, cols], sh_buf.at[third, :, cols], sf_recv.at[c]
+        ).wait()
+    part = shared_ref.shape[0] // 3
+    normed = normed_ref[...]
+    hidden_parts = []
+    for blk in range(n_tp):
+        g = lax.dot_general(normed, sh_buf[blk, 0:part, :], contract, preferred_element_type=F32)
+        u = lax.dot_general(
+            normed, sh_buf[blk, part : 2 * part, :], contract, preferred_element_type=F32
+        )
+        hidden_parts.append(((g / (1.0 + jnp.exp(-g))) * u).astype(BF16))
+    narrow = wide // 2
+    for c in range(2 * CHUNKS):
+        cols = slice(c * narrow, (c + 1) * narrow)
+        total = jnp.zeros((normed.shape[0], narrow), F32)
+        for blk in range(n_tp):
+            piece = jnp.dot(
+                hidden_parts[blk],
+                sh_buf[blk, 2 * part : 3 * part, cols],
+                preferred_element_type=F32,
+            )
+            total += piece.astype(BF16).astype(F32)
+        sh_out[:, cols] = total.astype(BF16)
+
+    for c in range(CHUNKS):
+        pltpu.make_async_copy(
+            r_buf.at[c, pl.ds(0, peer_rows)], r_buf.at[c, pl.ds(0, peer_rows)], y_recv.at[c]
+        ).wait()
+        pltpu.make_async_copy(
+            r_buf.at[c, pl.ds(0, group)], r_buf.at[c, pl.ds(0, group)], y_own.at[c]
+        ).wait()
+        back = r_buf[c]
+        routed = jnp.dot(high_ref[...], back, preferred_element_type=F32) + jnp.dot(
+            low_ref[...], back, preferred_element_type=F32
+        )
+        cols = slice(c * wide, (c + 1) * wide)
+        res_ref[:, cols] = (sh_out[:, cols].astype(F32) + routed).astype(BF16)
+
+    for c in range(CHUNKS):
+        pltpu.make_async_copy(
+            x_buf.at[c, pl.ds(0, peer_rows)], x_buf.at[c, pl.ds(0, peer_rows)], x_send.at[c]
+        ).wait()
+        pltpu.make_async_copy(
+            y_buf.at[c, pl.ds(0, peer_rows)], y_buf.at[c, pl.ds(0, peer_rows)], y_send.at[c]
+        ).wait()
+        shared_first(mate, 0, c).wait_send()
+        shared_first(across, 1, c).wait_send()
+        across_copies[c].wait_send()
+    for step in range(n_ep - 1):
+
+        @pl.when((e_pos - step >= 0) & (e_pos + 1 < n_ep))
+        def _():
+            for copy in kv_copy(step, kn_ref, v_ref):
+                copy.wait_send()
+
+
+def fused_local(n_ep, n_tp, *args):
+    (
+        queries,
+        key_vectors,
+        values,
+        forget_cum,
+        query_gain,
+        key_gain,
+        tokens,
+        norm_gain,
+        routes,
+        route_weights,
+        expert_gate,
+        expert_up,
+        expert_down,
+        shared_gate,
+        shared_up,
+        shared_down,
+    ) = args
+    rows, heads, size = queries.shape
+    row_count, dim = tokens.shape
+    local_count, _, hidden = expert_gate.shape
+    count = n_ep * n_tp
+    slots = count * local_count * CAP
+    part = shared_gate.shape[1]
+    flat = heads * size
+    vmem = pl.BlockSpec(memory_space=pltpu.VMEM)
+    hbm = pl.BlockSpec(memory_space=pltpu.HBM)
+    sds = jax.ShapeDtypeStruct
+    normed, outgoing, high, low, query_norm, key_norm = pl.pallas_call(
+        functools.partial(prepare_kernel, local_count, heads),
+        out_shape=(
+            sds((row_count, dim), BF16),
+            sds((slots, dim), BF16),
+            sds((row_count, slots), BF16),
+            sds((row_count, slots), BF16),
+            sds((rows, flat), BF16),
+            sds((rows, flat), BF16),
+        ),
+        in_specs=[vmem] * 9,
+        out_specs=[vmem] * 6,
+        name="prepare",
+    )(
+        tokens,
+        norm_gain.reshape(1, dim),
+        routes,
+        routes.T,
+        route_weights,
+        queries.reshape(rows, flat),
+        key_vectors.reshape(rows, flat),
+        query_gain.reshape(1, size),
+        key_gain.reshape(1, size),
+    )
+    shared = jnp.concatenate([shared_gate.T, shared_up.T, shared_down], axis=0)
+    query_cum = lax.dynamic_slice_in_dim(forget_cum, lax.axis_index("ep") * rows, rows, 0)
+    wide = dim // CHUNKS
+    dma = pltpu.SemaphoreType.DMA
+    attended, routed = pl.pallas_call(
+        functools.partial(fused_kernel, n_ep, n_tp, heads),
+        out_shape=(sds((rows, flat), BF16), sds((row_count, dim), BF16)),
+        in_specs=[vmem] * 6 + [hbm] * 7,
+        out_specs=[vmem] * 2,
+        scratch_shapes=[
+            pltpu.VMEM((CHUNKS, slots, wide), BF16),
+            pltpu.VMEM((CHUNKS, slots, wide), BF16),
+            pltpu.VMEM((CHUNKS, slots, wide), BF16),
+            pltpu.VMEM((SLOTS, 2, wide, hidden), BF16),
+            pltpu.VMEM((local_count * hidden, dim), BF16),
+            pltpu.VMEM((n_tp, 3 * part, dim), BF16),
+            pltpu.VMEM((n_ep, 2, rows, flat), BF16),
+            pltpu.VMEM((slots, hidden), F32),
+            pltpu.VMEM((slots, hidden), F32),
+            pltpu.VMEM((slots, local_count * hidden), BF16),
+            pltpu.VMEM((row_count, dim), BF16),
+            dma((CHUNKS,)),
+            dma((CHUNKS,)),
+            dma((CHUNKS,)),
+            dma((CHUNKS,)),
+            dma((CHUNKS,)),
+            dma((CHUNKS,)),
+            dma((SLOTS, 2)),
+            dma,
+            dma((2, CHUNKS)),
+            dma((2, CHUNKS)),
+            dma,
+            dma((CHUNKS,)),
+            dma((CHUNKS,)),
+            dma((n_ep - 1, 2)),
+            dma((n_ep - 1, 2)),
+            dma((2,)),
+        ],
+        compiler_params=pltpu.CompilerParams(
+            collective_id=0, has_side_effects=True, vmem_limit_bytes=60 * 1024 * 1024
+        ),
+        name="fused",
+    )(
+        normed,
+        high,
+        low,
+        query_norm,
+        query_cum,
+        forget_cum.T,
+        outgoing,
+        key_norm,
+        values.reshape(rows, flat),
+        expert_gate,
+        expert_up,
+        expert_down.reshape(local_count * hidden, dim),
+        shared,
+    )
+    return attended.reshape(rows, heads, size), routed
+
+
+def local_of(mesh):
+    n_ep, n_tp = mesh.shape["ep"], mesh.shape["tp"]
+
+    def run(*args):
+        experts = args[10]
+        group = CAP * experts.shape[0]
+        if n_tp == 4 and n_ep == 4 and group % 16 == 0 and args[15].shape[0] % 16 == 0:
+            return fused_local(n_ep, n_tp, *args)
+        return local(*args)
+
+    return run
+
+
 def solution(mesh):
     placed = (
         P(("grp", "ep"), "tp", None),
@@ -185,7 +769,7 @@
         P("tp", None),
     )
     return jax.shard_map(
-        local,
+        local_of(mesh),
         mesh=mesh,
         in_specs=placed,
         out_specs=(P(("grp", "ep"), "tp", None), P(("grp", "ep", "tp"), None)),

time: 231 us -> 139 us (0.60)
  Pallas kernels: 0 us -> 123 us
  blocking collectives: 73.5 us -> 0 us
  waiting for transfers between devices: 41.3 us -> 0 us
  matrix products: 39.7 us -> 0 us
  starting transfers between devices: 19.4 us -> 0 us
  other arithmetic: 18.3 us -> 2.37 us
  between operations: 14.1 us -> 0.65 us
  local copies, waits for them, and re-layouts: 24.6 us -> 11.4 us
    pallas_call x0 -> x2, Pallas kernels: none -> 123 us  [the longest x1 119 us: fused_local(): pl.pallas_call(functools.partial(fused_kernel, n_ep, n_tp, heads), out_sh...]
    all_gather x2 -> x0, blocking collectives: 73.5 us -> none  [the longest x1 57.6 us: attend(): key_part = lax.all_gather(key_norm, 'ep', axis=0, tiled=True)]
    dot_general x7 -> x0, matrix products: 39.7 us -> none  [the longest x1 21.4 us: mixture(): jnp.einsum('csef,efd->csed', hidden, expert_down, preferred_element_type=...]
    all_to_all x2 -> x0, waiting for transfers between devices: 39.6 us -> none  [the longest x1 39.6 us: mixture(): lax.all_to_all(outgoing, ('ep', 'tp'), split_axis=1, concat_axis=1, tiled...]
    all_to_all x2 -> x0, starting transfers between devices: 18.9 us -> none  [the longest x1 11.5 us: mixture(): lax.all_to_all(produced, ('ep', 'tp'), split_axis=1, concat_axis=1, tiled...]
    reduce_sum x7 -> x0, other arithmetic: 11.2 us -> none  [the longest x1 8.75 us: mixture(): jnp.sum(route_weights[:, :, None] * picked_rows.astype(jnp.float32), axis=1)]
    convert_element_type x2 -> x0, local copies, waits for them, and re-layouts: 8.18 us -> none  [the longest x1 5.44 us: mixture(): picked_rows.astype(jnp.float32)]
    unnamed x26 -> x5, local copies, waits for them, and re-layouts: 1.06 us -> 7.39 us
  transfers between devices with their start and end apart: 5 -> 0, of which waited for: 1 -> 0; matrix products, arithmetic and copies ran while one was open for 22% -> 0% of each run, Pallas kernels for 0% -> 0%
where the time goes in v1:
time: 139 us; the launch traced here: 138 us
  Pallas kernels  123 us (88%)
  local copies, waits for them, and re-layouts  11.4 us (8%)
  other arithmetic  2.37 us (2%)
    pallas_call x1, Pallas kernels, fused_local(): pl.pallas_call(functools.partial(fused_kernel, n_ep, n_tp, heads), out_sh...  119 us
    unnamed x5, local copies, waits for them, and re-layouts  7.39 us
    pallas_call x1, Pallas kernels, fused_local(): pl.pallas_call(functools.partial(prepare_kernel, local_count, heads), out...  3.94 us

profile of v1, /device:TPU:0, one launch (start us, length us, event | category | flops | bytes accessed | tf_op | source)
XLA Modules:
  0.0 137.6 jit_solution(4754452371420990129)
XLA Ops:
  0.6 0.7 constant_dynamic-slice_fusion
  1.3 0.7 copy.21.qc_ref
  2.1 1.4 %copy.19.weights_ref = f32[128,2]{1,0:T(8,128)} copy(f32[128,2]{0,1:T(2,128)} %param.25) | data formatting | bytes 2048 | tf_op args[9]
  3.5 1.4 %copy.18.routes_ref = s32[128,2]{1,0:T(8,128)} copy(s32[128,2]{0,1:T(2,128)} %param.24) | data formatting | bytes 2048 | tf_op args[8]
  4.9 1.6 %copy.28 = bf16[16,8,4,128]{3,1,2,0:T(8,128)(2,1)} copy(bf16[16,8,4,128]{3,2,1,0:T(4,128)(2,1)} %bitcast.22) | data formatting | bytes 262144
  6.4 1.7 %copy_bitcast_fusion.1 = (bf16[128,512]{1,0:T(8,128)(2,1)}, bf16[128,512]{1,0:T(8,128)(2,1)}) fusion(bf16[16,8,4,128]{3,2,1,0:T(4,128)(2,1)} %bitcast.23, bf16[16,8,4,128]{3,2,1,0:T(4,128)(2,1)} %bitcast.24), kind=kLoop, calls=%fused_computation.2 | loop fusion | bytes 524288 | tf_op jit(solution)/shard_map/reshape | solution.py:675
  8.1 2.4 %pad_maximum_fusion.shared_ref = bf16[144,4096]{1,0:T(8,128)(2,1)} fusion(bf16[48,4096]{1,0:T(8,128)(2,1)} %param.31, bf16[48,4096]{1,0:T(8,128)(2,1)} %bitcast.20, bf16[48,4096]{1,0:T(8,128)(2,1)} %bitcast.21), kind=kLoop, calls=%fused_computation | loop fusion | flops 3538944 | bytes 2359296 | tf_op jit(solution)/shard_map/concatenate | solution.py:679
  10.5 3.9 %prepare.1 = (bf16[128,4096]{1,0:T(8,128)(2,1)}, bf16[256,4096]{1,0:T(8,128)(2,1)}, bf16[128,256]{1,0:T(8,128)(2,1)}, bf16[128,256]{1,0:T(8,128)(2,1)}, bf16[128...) custom-call(bf16[128,4096]{1,0:T(8,128)(2,1)} %tokens_ref.1, f32[1,4096]{1,0:T(1,128)} %bitcast.25, s32[128,2]{1,0:T(8,128)} %copy.18.routes_ref, ...), custom_call_target="tpu_custom_call" | custom-call | tf_op jit(solution)/shard_map/prepare/pallas_call | solution.py:655
  14.4 119.3 %fused.1 = (bf16[128,512]{1,0:T(8,128)(2,1)}, bf16[128,4096]{1,0:T(8,128)(2,1)}) custom-call(bf16[128,4096]{1,0:T(8,128)(2,1)} %get-tuple-element.10.normed_ref, bf16[128,256]{1,0:T(8,128)(2,1)} %get-tuple-element.11.high_ref, bf16[128,256]{1,0:T(8,128)(2,1)} %get-tuple-element.12.low_ref, bf16[128,512]{1,0:T(8,128)(2,1)} %get-tuple-element.13.qn_ref, ...), custom_call_target="tpu_custom_call" | custom-call | tf_op jit(solution)/shard_map/fused/pallas_call | solution.py:683
  133.8 1.6 %reshape.35 = bf16[128,4,128]{2,1,0:T(4,128)(2,1)} reshape(bf16[128,512]{1,0:T(8,128)(2,1)} %get-tuple-element.16) | data formatting | bytes 262144 | tf_op jit(solution)/shard_map/reshape | solution.py:736
  135.4 2.3 %copy.30 = bf16[128,4096]{1,0:T(8,128)(2,1)} copy(bf16[128,4096]{1,0:T(8,128)(2,1)} %get-tuple-element.23) | data formatting | bytes 2097152
